TPU v7x, 32 devices: a whole 2x2x4 slice. The times are simulated.
32 devices in a mesh: fs: 8 (over z, x), tp: 4 (over y, core).
Axes of the slice: x: 2, y: 2, z: 4, core: 2. Of those that a mesh axis runs over, the one named last changes fastest.
Arguments:
- inputs: bfloat16 [8192, 2048], P('fs'), may hold values from -6 to 6
- cotangents: bfloat16 [8192, 3, 1024], P('fs', None, 'tp'), may hold values from -0.06591797 to 0.06591797
- factors: bfloat16 [3, 2048, 256], P(None, 'fs'), may hold values from -13.810679 to 13.810679
- first_moment: float32 [3, 256, 1024], P(None, None, 'tp'), may hold values from -6 to 6
- second_moment: float32 [3, 256, 1024], P(None, None, 'tp'), may hold values from 0.05 to 1
- master: float32 [3, 2048, 1024], P(None, 'fs', 'tp'), may hold values from -0.125 to 0.125
Outputs:
- update_step: float32 [3, 2048, 1024], P(None, 'fs', 'tp')
- new_master: float32 [3, 2048, 1024], P(None, 'fs', 'tp')
- new_copy: bfloat16 [3, 2048, 1024], P(None, None, 'tp')
- new_first: float32 [3, 256, 1024], P(None, None, 'tp')
- new_second: float32 [3, 256, 1024], P(None, None, 'tp')
All inputs are finite; a program needn't handle non-finite values.
Results may differ from a plain program's by a relative error of at most 0.001.
Values may be sent and summed in bfloat16 or wider, within the bound.
A program may use at most 64 MiB of HBM per device.

v0:
```python
import jax
import jax.numpy as jnp
from jax import lax
from jax.sharding import PartitionSpec as P

D = 2048
MW = 1024
beta_first = 0.8
beta_second = 0.9
adam_eps = 1e-08
norm_eps = 1e-06
learning_rate = 0.005


def local(inputs, cotangents, factors, first_moment, second_moment, master):
    factor32 = factors.astype(jnp.float32)
    lowered = jnp.einsum(
        "tk,mkr->mtr",
        inputs,
        lax.all_gather(factors, "fs", axis=1, tiled=True),
        preferred_element_type=jnp.float32,
    )
    cot_wide = cotangents.astype(jnp.float32)
    partial_value = jnp.einsum("mtr,tmc->mrc", lowered, cot_wide, precision=lax.Precision.HIGHEST)
    projected = lax.psum(partial_value, "fs")
    new_first = beta_first * first_moment + (1.0 - beta_first) * projected
    new_second = beta_second * second_moment + (1.0 - beta_second) * projected * projected
    normed = new_first / (jnp.sqrt(new_second) + adam_eps)
    update = jnp.einsum("mdr,mrc->mdc", factor32, normed, precision=lax.Precision.HIGHEST)
    squares = lax.psum(jnp.sum(update * update, axis=(1, 2)), ("fs", "tp"))
    root_mean = jnp.sqrt(squares / (D * MW) + norm_eps)
    update_step = update / root_mean[:, None, None]
    new_master = master - learning_rate * update_step
    new_copy = lax.all_gather(new_master.astype(jnp.bfloat16), "fs", axis=1, tiled=True)
    return (update_step, new_master, new_copy, new_first, new_second)


def solution(mesh):
    placed = (
        P("fs", None),
        P("fs", None, "tp"),
        P(None, "fs", None),
        P(None, None, "tp"),
        P(None, None, "tp"),
        P(None, "fs", "tp"),
    )
    return jax.shard_map(
        local,
        mesh=mesh,
        in_specs=placed,
        out_specs=(
            P(None, "fs", "tp"),
            P(None, "fs", "tp"),
            P(None, None, "tp"),
            P(None, None, "tp"),
            P(None, None, "tp"),
        ),
        check_vma=False,
    )
```

profile of v0, /device:TPU:0, one launch (start us, length us, event | category | flops | bytes accessed | tf_op | source)
XLA Modules:
  0.0 275.3 jit_solution(5420966089030130023)
XLA Ops:
  7.2 0.0 copy-start
  7.2 0.0 all-gather.3.cloned.1.call-start
  7.2 0.7 all-gather.3.cloned.1.call-update
  7.9 0.0 all-reduce.2.cloned.1.call-start
  8.0 65.0 %all-gather.3.cloned.1.call-done = bf16[3,2048,256]{2,1,0:T(8,128)(2,1)} async-done(((bf16[3,256,256]{2,1,0:T(8,128)(2,1)}), bf16[3,2048,256]{2,1,0:T(8,128)(2,1)}) %all-gather.3.cloned.1.call-update) | async-done | bytes 3145744 | tf_op jit(solution)/shard_map/all_gather | solution.py:20
  72.9 6.2 %fusion = f32[3,256,1024]{2,1,0:T(8,128)S(1)} fusion(bf16[3,2048,256]{2,1,0:T(8,128)(2,1)} %all-gather.3.cloned.1.call-done, bf16[1024,2048]{1,0:T(8,128)(2,1)} %param.6), kind=kOutput, calls=%fused_computation | convolution fusion | flops 3221225472 | bytes 10485760 | tf_op jit(solution)/shard_map/tk,mkr->mtr/dot_general | solution.py:17
  79.2 0.0 copy-done
  79.2 0.0 copy-start.1
  79.2 2.5 fusion.10
  81.7 0.0 copy-start.4
  81.7 0.0 all-reduce.2.cloned.1.call-update
  81.7 0.0 all-gather.5.cloned.1.call-start
  81.7 0.0 copy-done.1
  81.8 0.3 copy.12
  82.0 73.5 %all-reduce.2.cloned.1.call-done = f32[3,256,256]{2,1,0:T(8,128)} async-done(((f32[3,256,256]{2,1,0:T(8,128)}), f32[3,256,256]{2,1,0:T(8,128)}) %all-reduce.2.cloned.1.call-update) | async-done | bytes 786448 | tf_op jit(solution)/shard_map/psum | solution.py:25
  155.6 1.8 fusion.2
  157.4 0.0 copy-start.2
  157.4 0.0 copy-start.3
  157.4 0.9 copy-done.2
  158.3 0.0 copy-done.4
  158.3 1.8 multiply_reduce_fusion
  160.1 0.0 copy-done.3
  160.1 39.4 %psum.15 = f32[3]{0:T(128)S(1)} all-reduce(f32[3]{0:T(128)S(1)} %get-tuple-element.15), channel_id=1, replica_groups=mesh['fs'=8,'tp'=4] {'fs','tp'}, use_global_device_ids=true, to_apply=%region_2.0 | all-reduce | flops 3 | bytes 24 | tf_op jit(solution)/shard_map/psum | solution.py:30
  199.6 2.4 fusion.9
  202.0 0.0 all-gather.5.cloned.1.call-update
  202.0 2.3 copy.14
  204.3 1.1 copy.13
  205.4 58.7 %all-gather.5.cloned.1.call-done = bf16[3,2048,256]{1,2,0:T(8,128)(2,1)} async-done(((bf16[3,256,256]{1,2,0:T(8,128)(2,1)}), bf16[3,2048,256]{1,2,0:T(8,128)(2,1)}) %all-gather.5.cloned.1.call-update) | async-done | bytes 3145744 | tf_op jit(solution)/shard_map/all_gather | solution.py:34
  264.2 4.6 %copy.15 = bf16[3,2048,256]{2,1,0:T(8,128)(2,1)} copy(bf16[3,2048,256]{1,2,0:T(8,128)(2,1)} %all-gather.5.cloned.1.call-done) | data formatting | bytes 6291456
  (1 shorter events, 0.0 us)
Async XLA Ops:
  7.2 72.0 %copy-start = (bf16[1024,3,256]{2,0,1:T(8,128)(2,1)S(1)}, bf16[1024,3,256]{2,0,1:T(8,128)(2,1)}, u32[]{:S(2)}) copy-start(bf16[1024,3,256]{2,0,1:T(8,128)(2,1)} %param.7) | copy-start | bytes 4718596
  7.2 65.8 %all-gather.3.cloned.1.call-start = ((), (), s32[]{:S(2)}) async-start(), calls=%async_computation | async-start | bytes 3538944 | tf_op jit(solution)/shard_map/all_gather | solution.py:20
  7.9 147.7 %all-reduce.2.cloned.1.call-start = ((), (), s32[]{:S(2)}) async-start(), calls=%async_computation.1 | async-start | bytes 1572864 | tf_op jit(solution)/shard_map/psum | solution.py:25
  79.2 2.6 copy-start.1
  81.7 76.6 %copy-start.4 = (bf16[3,256,256]{2,1,0:T(8,128)(2,1)S(1)}, bf16[3,256,256]{2,1,0:T(8,128)(2,1)}, u32[]{:S(2)}) copy-start(bf16[3,256,256]{2,1,0:T(8,128)(2,1)} %param.8) | copy-start | bytes 1179652
  81.7 182.5 %all-gather.5.cloned.1.call-start = ((), (), s32[]{:S(2)}) async-start(), calls=%async_computation.2 | async-start | bytes 3538944 | tf_op jit(solution)/shard_map/all_gather | solution.py:34
  157.4 0.9 copy-start.2
  157.4 2.7 copy-start.3
Sparse Core Ops, SparseCore 0:
  10.2 62.7 all-gather.2
  81.8 73.7 all-reduce.1
  202.1 62.0 all-gather.4
where the time goes:
time: 276 us; the launch traced here: 275 us
  waiting for transfers between devices  198 us (72%)
  blocking collectives  39.4 us (14%)
  between operations  13.8 us (5%)
  matrix products  10.5 us (4%)
  local copies, waits for them, and re-layouts  9.21 us (3%)
  other arithmetic  4.22 us (2%)
    psum x1, waiting for transfers between devices, local(): projected = lax.psum(partial_value, 'fs')  73.5 us
    all_gather x1, waiting for transfers between devices, local(): lax.all_gather(factors, 'fs', axis=1, tiled=True)  65 us
    all_gather x1, waiting for transfers between devices, local(): lax.all_gather(new_master.astype(jnp.bfloat16), 'fs', axis=1, tiled=True)  58.7 us
    psum x1, blocking collectives, local(): squares = lax.psum(jnp.sum(update * update, axis=(1, 2)), ('fs', 'tp'))  39.4 us
    unnamed x14, local copies, waits for them, and re-layouts  9.21 us
    dot_general x1, matrix products, local(): jnp.einsum('tk,mkr->mtr', inputs, lax.all_gather(factors, 'fs', axis=1, t...  6.22 us
  transfers between devices with their start and end apart: 3, of which 3 were waited for; matrix products, arithmetic and copies ran while one was open for 1% of the time, Pallas kernels for 0%

commit v1 on v0

--- a/solution.py
+++ b/solution.py
@@ -27,7 +27,9 @@
     new_second = beta_second * second_moment + (1.0 - beta_second) * projected * projected
     normed = new_first / (jnp.sqrt(new_second) + adam_eps)
     update = jnp.einsum("mdr,mrc->mdc", factor32, normed, precision=lax.Precision.HIGHEST)
-    squares = lax.psum(jnp.sum(update * update, axis=(1, 2)), ("fs", "tp"))
+    squares = jnp.sum(update * update, axis=(1, 2))
+    for axis in ("tp", "fs"):
+        squares = lax.psum(squares, axis)
     root_mean = jnp.sqrt(squares / (D * MW) + norm_eps)
     update_step = update / root_mean[:, None, None]
     new_master = master - learning_rate * update_step

time: 276 us -> 260 us (0.942)
  blocking collectives: 39.4 us -> 25.2 us
    psum x1 -> x2, blocking collectives: 39.4 us -> 25.2 us  [local(): squares = lax.psum(squares, axis)]
    unnamed x14 -> x16, local copies, waits for them, and re-layouts: 9.21 us -> 8.97 us
where the time goes in v1:
time: 260 us
  waiting for transfers between devices  198 us (76%)
  blocking collectives  25.2 us (10%)
  between operations  13.8 us (5%)
  matrix products  10.5 us (4%)
  local copies, waits for them, and re-layouts  8.97 us (3%)
  other arithmetic  3.97 us (2%)
    psum x1, waiting for transfers between devices, local(): projected = lax.psum(partial_value, 'fs')  73.8 us
    all_gather x1, waiting for transfers between devices, local(): lax.all_gather(factors, 'fs', axis=1, tiled=True)  65 us
    all_gather x1, waiting for transfers between devices, local(): lax.all_gather(new_master.astype(jnp.bfloat16), 'fs', axis=1, tiled=True)  58 us
    psum x2, blocking collectives, local(): squares = lax.psum(squares, axis)  25.2 us
    unnamed x16, local copies, waits for them, and re-layouts  8.97 us
    dot_general x1, matrix products, local(): jnp.einsum('tk,mkr->mtr', inputs, lax.all_gather(factors, 'fs', axis=1, t...  6.22 us
  transfers between devices with their start and end apart: 3, of which 3 were waited for; matrix products, arithmetic and copies ran while one was open for 1% of the time, Pallas kernels for 0%

profile of v1, /device:TPU:0, one launch (start us, length us, event | category | flops | bytes accessed | tf_op | source)
XLA Modules:
  0.0 260.1 jit_solution(15907734993542520646)
XLA Ops:
  7.2 0.0 copy-start
  7.2 0.0 all-gather.3.cloned.1.call-start
  7.2 0.7 all-gather.3.cloned.1.call-update
  7.9 0.0 all-reduce.2.cloned.1.call-start
  8.0 65.0 %all-gather.3.cloned.1.call-done = bf16[3,2048,256]{2,1,0:T(8,128)(2,1)} async-done(((bf16[3,256,256]{2,1,0:T(8,128)(2,1)}), bf16[3,2048,256]{2,1,0:T(8,128)(2,1)}) %all-gather.3.cloned.1.call-update) | async-done | bytes 3145744 | tf_op jit(solution)/shard_map/all_gather | solution.py:20
  72.9 6.2 %fusion = f32[3,256,1024]{2,1,0:T(8,128)S(1)} fusion(bf16[3,2048,256]{2,1,0:T(8,128)(2,1)} %all-gather.3.cloned.1.call-done, bf16[1024,2048]{1,0:T(8,128)(2,1)} %param.6), kind=kOutput, calls=%fused_computation | convolution fusion | flops 3221225472 | bytes 10485760 | tf_op jit(solution)/shard_map/tk,mkr->mtr/dot_general | solution.py:17
  79.2 0.0 copy-done
  79.2 0.0 copy-start.2
  79.2 2.5 fusion.10
  81.7 0.0 copy-start.5
  81.7 0.0 all-reduce.2.cloned.1.call-update
  81.7 0.0 copy-start.1
  81.7 0.0 all-gather.5.cloned.1.call-start
  81.8 73.8 %all-reduce.2.cloned.1.call-done = f32[3,256,256]{2,1,0:T(8,128)} async-done(((f32[3,256,256]{2,1,0:T(8,128)}), f32[3,256,256]{2,1,0:T(8,128)}) %all-reduce.2.cloned.1.call-update) | async-done | bytes 786448 | tf_op jit(solution)/shard_map/psum | solution.py:25
  155.6 0.0 copy-done.2
  155.6 1.6 fusion.2
  157.2 0.0 copy-start.3
  157.2 0.0 copy-start.4
  157.2 0.9 copy-done.3
  158.1 0.0 copy-done.5
  158.1 1.8 multiply_reduce_fusion
  159.9 0.0 copy-done.4
  159.9 5.6 %psum.22 = f32[3]{0:T(128)S(1)} all-reduce(f32[3]{0:T(128)S(1)} %get-tuple-element.15), channel_id=1, replica_groups=mesh['fs'=8,'tp'=4] {'tp'}, use_global_device_ids=true, to_apply=%region_2.0 | all-reduce | flops 3 | bytes 24 | tf_op jit(solution)/shard_map/psum | solution.py:32
  165.5 0.0 copy-done.1
  165.5 1.1 copy.12
  166.7 19.6 %psum.23 = f32[3]{0:T(128)S(1)} all-reduce(f32[3]{0:T(128)S(1)} %psum.22), channel_id=1, replica_groups=mesh['fs'=8,'tp'=4] {'fs'}, use_global_device_ids=true, to_apply=%region_3.0 | all-reduce | flops 3 | bytes 24 | tf_op jit(solution)/shard_map/psum | solution.py:32
  186.3 2.4 fusion.9
  188.6 0.0 all-gather.5.cloned.1.call-update
  188.7 1.1 copy.14
  189.8 1.1 copy.13
  191.0 58.0 %all-gather.5.cloned.1.call-done = bf16[3,2048,256]{1,2,0:T(8,128)(2,1)} async-done(((bf16[3,256,256]{1,2,0:T(8,128)(2,1)}), bf16[3,2048,256]{1,2,0:T(8,128)(2,1)}) %all-gather.5.cloned.1.call-update) | async-done | bytes 3145744 | tf_op jit(solution)/shard_map/all_gather | solution.py:36
  249.0 4.6 %copy.15 = bf16[3,2048,256]{2,1,0:T(8,128)(2,1)} copy(bf16[3,2048,256]{1,2,0:T(8,128)(2,1)} %all-gather.5.cloned.1.call-done) | data formatting | bytes 6291456
  (1 shorter events, 0.0 us)
Async XLA Ops:
  7.2 72.0 %copy-start = (bf16[1024,3,256]{2,0,1:T(8,128)(2,1)S(1)}, bf16[1024,3,256]{2,0,1:T(8,128)(2,1)}, u32[]{:S(2)}) copy-start(bf16[1024,3,256]{2,0,1:T(8,128)(2,1)} %param.7) | copy-start | bytes 4718596
  7.2 65.8 %all-gather.3.cloned.1.call-start = ((), (), s32[]{:S(2)}) async-start(), calls=%async_computation | async-start | bytes 3538944 | tf_op jit(solution)/shard_map/all_gather | solution.py:20
  7.9 147.7 %all-reduce.2.cloned.1.call-start = ((), (), s32[]{:S(2)}) async-start(), calls=%async_computation.1 | async-start | bytes 1572864 | tf_op jit(solution)/shard_map/psum | solution.py:25
  79.2 76.4 %copy-start.2 = (f32[3,256,256]{2,1,0:T(8,128)S(1)}, f32[3,256,256]{2,1,0:T(8,128)}, u32[]{:S(2)}) copy-start(f32[3,256,256]{2,1,0:T(8,128)} %param.10) | copy-start | bytes 2359300
  81.7 76.4 %copy-start.5 = (bf16[3,256,256]{2,1,0:T(8,128)(2,1)S(1)}, bf16[3,256,256]{2,1,0:T(8,128)(2,1)}, u32[]{:S(2)}) copy-start(bf16[3,256,256]{2,1,0:T(8,128)(2,1)} %param.8) | copy-start | bytes 1179652
  81.7 83.8 %copy-start.1 = (f32[3,256,256]{2,1,0:T(8,128)S(1)}, f32[3,256,256]{2,1,0:T(8,128)}, u32[]{:S(2)}) copy-start(f32[3,256,256]{2,1,0:T(8,128)} %param.11) | copy-start | bytes 2359300
  81.7 167.2 %all-gather.5.cloned.1.call-start = ((), (), s32[]{:S(2)}) async-start(), calls=%async_computation.2 | async-start | bytes 3538944 | tf_op jit(solution)/shard_map/all_gather | solution.py:36
  157.2 0.9 copy-start.3
  157.2 2.7 %copy-start.4 = (f32[3,256,256]{2,1,0:T(8,128)}, f32[3,256,256]{2,1,0:T(8,128)S(1)}, u32[]{:S(2)}) copy-start(f32[3,256,256]{2,1,0:T(8,128)S(1)} %get-tuple-element.14) | copy-start | bytes 2359300
Sparse Core Ops, SparseCore 0:
  10.2 62.7 all-gather.2
  81.8 73.7 all-reduce.1
  188.8 60.1 all-gather.4

commit v2 on v0

--- a/solution.py
+++ b/solution.py
@@ -22,7 +22,8 @@
     )
     cot_wide = cotangents.astype(jnp.float32)
     partial_value = jnp.einsum("mtr,tmc->mrc", lowered, cot_wide, precision=lax.Precision.HIGHEST)
-    projected = lax.psum(partial_value, "fs")
+    shards = lax.all_gather(partial_value, "fs", axis=0, tiled=False)
+    projected = shards.sum(axis=0)
     new_first = beta_first * first_moment + (1.0 - beta_first) * projected
     new_second = beta_second * second_moment + (1.0 - beta_second) * projected * projected
     normed = new_first / (jnp.sqrt(new_second) + adam_eps)

time: 276 us -> 303 us (1.098)
  waiting for transfers between devices: 198 us -> 223 us
  other arithmetic: 4.22 us -> 7.33 us
    all_gather x0 -> x1, waiting for transfers between devices: none -> 97.2 us  [local(): shards = lax.all_gather(partial_value, 'fs', axis=0, tiled=False)]
    psum x1 -> x0, waiting for transfers between devices: 73.5 us -> none  [local(): projected = lax.psum(partial_value, 'fs')]
    reduce_sum x0 -> x1, other arithmetic: none -> 3.29 us  [local(): projected = shards.sum(axis=0)]
where the time goes in v2:
time: 303 us; the launch traced here: 302 us
  waiting for transfers between devices  223 us (74%)
  blocking collectives  38.3 us (13%)
  between operations  13.8 us (5%)
  matrix products  10.5 us (3%)
  local copies, waits for them, and re-layouts  9.21 us (3%)
  other arithmetic  7.33 us (2%)
    all_gather x1, waiting for transfers between devices, local(): shards = lax.all_gather(partial_value, 'fs', axis=0, tiled=False)  97.2 us
    all_gather x1, waiting for transfers between devices, local(): lax.all_gather(factors, 'fs', axis=1, tiled=True)  65 us
    all_gather x1, waiting for transfers between devices, local(): lax.all_gather(new_master.astype(jnp.bfloat16), 'fs', axis=1, tiled=True)  60.1 us
    psum x1, blocking collectives, local(): squares = lax.psum(jnp.sum(update * update, axis=(1, 2)), ('fs', 'tp'))  38.3 us
    unnamed x14, local copies, waits for them, and re-layouts  9.21 us
    dot_general x1, matrix products, local(): jnp.einsum('tk,mkr->mtr', inputs, lax.all_gather(factors, 'fs', axis=1, t...  6.22 us
  transfers between devices with their start and end apart: 3, of which 3 were waited for; matrix products, arithmetic and copies ran while one was open for 1% of the time, Pallas kernels for 0%

profile of v2, /device:TPU:0, one launch (start us, length us, event | category | flops | bytes accessed | tf_op | source)
XLA Modules:
  0.0 302.3 jit_solution(14630784286230721568)
XLA Ops:
  7.2 0.0 copy-start
  7.2 0.0 all-gather.5.cloned.1.call-start
  7.2 0.7 all-gather.5.cloned.1.call-update
  7.9 0.0 all-gather.9.cloned.1.call-start
  8.0 65.0 %all-gather.5.cloned.1.call-done = bf16[3,2048,256]{2,1,0:T(8,128)(2,1)} async-done(((bf16[3,256,256]{2,1,0:T(8,128)(2,1)}), bf16[3,2048,256]{2,1,0:T(8,128)(2,1)}) %all-gather.5.cloned.1.call-update) | async-done | bytes 3145744 | tf_op jit(solution)/shard_map/all_gather | solution.py:20
  72.9 6.2 %fusion = f32[3,256,1024]{2,1,0:T(8,128)S(1)} fusion(bf16[3,2048,256]{2,1,0:T(8,128)(2,1)} %all-gather.5.cloned.1.call-done, bf16[1024,2048]{1,0:T(8,128)(2,1)} %param.6), kind=kOutput, calls=%fused_computation | convolution fusion | flops 3221225472 | bytes 10485760 | tf_op jit(solution)/shard_map/tk,mkr->mtr/dot_general | solution.py:17
  79.2 0.0 copy-done
  79.2 0.0 copy-start.1
  79.2 2.5 fusion.10
  81.7 0.0 all-gather.9.cloned.1.call-update
  81.7 0.0 all-gather.7.cloned.1.call-start
  81.7 0.0 copy-done.1
  81.8 0.3 copy.17
  82.0 97.2 %all-gather.9.cloned.1.call-done = f32[24,256,256]{2,1,0:T(8,128)} async-done(((f32[3,256,256]{2,1,0:T(8,128)}), f32[24,256,256]{2,1,0:T(8,128)}) %all-gather.9.cloned.1.call-update) | async-done | bytes 6291472 | tf_op jit(solution)/shard_map/all_gather | solution.py:25
  179.2 3.3 %reduce_sum.18 = f32[3,256,256]{2,1,0:T(8,128)S(1)} reduce(f32[8,3,256,256]{3,2,1,0:T(8,128)} %bitcast.11, f32[]{:T(128)} %constant.2.clone.1), dimensions={0}, to_apply=%region_0.0 | reduce | flops 1376256 | bytes 7077892 | tf_op jit(solution)/shard_map/reduce_sum | solution.py:26
  182.5 0.0 copy-start.4
  182.5 1.6 fusion.2
  184.2 0.0 copy-start.2
  184.2 0.0 copy-start.3
  184.2 0.9 copy-done.2
  185.0 0.0 copy-done.4
  185.0 1.8 multiply_reduce_fusion
  186.9 0.0 copy-done.3
  186.9 38.3 %psum.7 = f32[3]{0:T(128)S(1)} all-reduce(f32[3]{0:T(128)S(1)} %get-tuple-element.20), channel_id=1, replica_groups=mesh['fs'=8,'tp'=4] {'fs','tp'}, use_global_device_ids=true, to_apply=%region_2.0 | all-reduce | flops 3 | bytes 24 | tf_op jit(solution)/shard_map/psum | solution.py:31
  225.2 2.4 fusion.9
  227.6 0.0 all-gather.7.cloned.1.call-update
  227.6 2.3 copy.19
  229.9 1.1 copy.18
  231.1 60.1 %all-gather.7.cloned.1.call-done = bf16[3,2048,256]{1,2,0:T(8,128)(2,1)} async-done(((bf16[3,256,256]{1,2,0:T(8,128)(2,1)}), bf16[3,2048,256]{1,2,0:T(8,128)(2,1)}) %all-gather.7.cloned.1.call-update) | async-done | bytes 3145744 | tf_op jit(solution)/shard_map/all_gather | solution.py:35
  291.1 4.6 %copy.20 = bf16[3,2048,256]{2,1,0:T(8,128)(2,1)} copy(bf16[3,2048,256]{1,2,0:T(8,128)(2,1)} %all-gather.7.cloned.1.call-done) | data formatting | bytes 6291456
  (1 shorter events, 0.0 us)
Async XLA Ops:
  7.2 72.0 %copy-start = (bf16[1024,3,256]{2,0,1:T(8,128)(2,1)S(1)}, bf16[1024,3,256]{2,0,1:T(8,128)(2,1)}, u32[]{:S(2)}) copy-start(bf16[1024,3,256]{2,0,1:T(8,128)(2,1)} %param.7) | copy-start | bytes 4718596
  7.2 65.8 %all-gather.5.cloned.1.call-start = ((), (), s32[]{:S(2)}) async-start(), calls=%async_computation | async-start | bytes 3538944 | tf_op jit(solution)/shard_map/all_gather | solution.py:20
  7.9 171.3 %all-gather.9.cloned.1.call-start = ((), (), s32[]{:S(2)}) async-start(), calls=%async_computation.2 | async-start | bytes 7077888 | tf_op jit(solution)/shard_map/all_gather | solution.py:25
  79.2 2.6 copy-start.1
  81.7 209.5 %all-gather.7.cloned.1.call-start = ((), (), s32[]{:S(2)}) async-start(), calls=%async_computation.1 | async-start | bytes 3538944 | tf_op jit(solution)/shard_map/all_gather | solution.py:35
  182.5 2.5 copy-start.4
  184.2 0.9 copy-start.2
  184.2 2.7 copy-start.3
Sparse Core Ops, SparseCore 0:
  10.2 62.7 all-gather.4
  81.8 97.3 all-gather.8
  227.8 63.3 all-gather.6
